TPU v7x, 32 devices: a whole 2x2x4 slice. The times are simulated.
32 devices in a mesh: grp: 2 (over x), ep: 16 (over z, y, core).
Axes of the slice: x: 2, y: 2, z: 4, core: 2. Of those that a mesh axis runs over, the one named last changes fastest.
Arguments:
- hidden: bfloat16 [96, 2048], P(('grp', 'ep')), parts along dimension 0, may hold values from -6 to 6
- conv_window: bfloat16 [96, 3, 6144], P(('grp', 'ep')), parts along dimension 0, may hold values from -6 to 6
- ssm_state: float32 [96, 64, 64, 128], P(('grp', 'ep')), parts along dimension 0, may hold values from -1.75 to 1.75
- gate_proj: bfloat16 [2048, 4096], P(None, 'ep'), may hold values from -0.125 to 0.125
- input_proj: bfloat16 [2048, 4096], P(None, 'ep'), may hold values from -0.125 to 0.125
- write_proj: bfloat16 [2048, 1024], P(None, 'ep'), may hold values from -0.125 to 0.125
- read_proj: bfloat16 [2048, 1024], P(None, 'ep'), may hold values from -0.125 to 0.125
- step_proj: bfloat16 [2048, 64], replicated, may hold values from -0.125 to 0.125
- step_bias: float32 [64], replicated, may hold values from -2 to 1
- decay_log: float32 [64], replicated, may hold values from -2.3 to 1.4
- decay_shift: float32 [96, 64], P(('grp', 'ep')), parts along dimension 0, may hold values from -0.7 to 0
- skip_scale: float32 [64], replicated, may hold values from -4 to 4
- conv_taps: bfloat16 [4, 6144], replicated, may hold values from -3 to 3
- conv_bias: float32 [6144], replicated, may hold values from -3 to 3
- mix_gain: float32 [2048], replicated, may hold values from 0.1 to 1.9
- group_gain: float32 [4096], replicated, may hold values from 0.1 to 1.9
- out_proj: bfloat16 [4096, 2048], P(None, 'ep'), may hold values from -0.09375 to 0.09375
- ffn_gain: float32 [2048], replicated, may hold values from 0.1 to 1.9
- router: bfloat16 [2048, 16], replicated, may hold values from -0.125 to 0.125
- expert_ids: int32 [96, 6], P(('grp', 'ep')), parts along dimension 0, may hold values from 0 to 15, all different within a row; in each aligned block of 3 rows (0 to 2, 3 to 5, ...) at most 2 rows name the same one
- expert_gate: bfloat16 [16, 2048, 512], P('ep'), may hold values from -0.125 to 0.125
- expert_up: bfloat16 [16, 2048, 512], P('ep'), may hold values from -0.125 to 0.125
- expert_down: bfloat16 [16, 512, 2048], P('ep'), may hold values from -0.25 to 0.25
- shared_gate: bfloat16 [2048, 512], P('ep'), may hold values from -0.125 to 0.125
- shared_up: bfloat16 [2048, 512], P('ep'), may hold values from -0.125 to 0.125
- shared_down: bfloat16 [512, 2048], replicated, may hold values from -0.25 to 0.25
Outputs:
- layer_out: bfloat16 [96, 2048], P(('grp', 'ep')), parts along dimension 0
- next_state: float32 [96, 64, 64, 128], P(('grp', 'ep')), parts along dimension 0
- next_window: bfloat16 [96, 3, 6144], P(('grp', 'ep')), parts along dimension 0
There are 2 independent parts, one for each index of `grp`. A program takes and returns all parts, laid end to end along the dimension named above; an argument that names none is the same for every part. Nothing has to cross between parts.
Inputs may be any that keep to these rules, and one draw needn't show every extreme that they name: `expert_ids`: each row names 6 different experts; in the rows of one device no expert is named by more than 2 rows, and in every draw some device's rows name some expert exactly 2 times.
All inputs are finite; a program needn't handle non-finite values.
Results may differ from a plain program's by a relative error of at most 0.019.
Values may be sent and summed in bfloat16 or wider, within the bound.
A program may use at most 128 MiB of HBM per device.

v0:
```python
import jax
import jax.numpy as jnp
from jax import lax
from jax.sharding import PartitionSpec as P

HEAD_DIM = 64
GROUPS = 8
STATE = 128
CAP = 2
epsilon = 1e-06
routed_scale = 2.5


def row_scale(values):
    return lax.rsqrt(jnp.mean(values * values, axis=-1, keepdims=True) + epsilon)


def matmul(left, right):
    return jnp.dot(left, right, preferred_element_type=jnp.float32)


def expert_result(rows_in, weight_gate, weight_up, weight_down):
    expert_hidden = (jax.nn.silu(matmul(rows_in, weight_gate)) * matmul(rows_in, weight_up)).astype(
        jnp.bfloat16
    )
    return matmul(expert_hidden, weight_down).astype(jnp.bfloat16)


def route_weights(routed_in, router, chosen):
    scores = jax.nn.sigmoid(matmul(routed_in, router))
    picked = jnp.take_along_axis(scores, chosen, axis=1)
    return routed_scale * picked / jnp.sum(picked, axis=1, keepdims=True)


def shards(
    hidden,
    conv_window,
    ssm_state,
    gate_proj,
    input_proj,
    write_proj,
    read_proj,
    step_proj,
    step_bias,
    decay_log,
    decay_shift,
    skip_scale,
    conv_taps,
    conv_bias,
    mix_gain,
    group_gain,
    out_proj,
    ffn_gain,
    router,
    expert_ids,
    expert_gate,
    expert_up,
    expert_down,
    shared_gate,
    shared_up,
    shared_down,
):
    local_rows = hidden.shape[0]
    device_index = lax.axis_index("ep")
    gathered = lax.all_gather(hidden, "ep", axis=0, tiled=True)
    gathered_wide = gathered.astype(jnp.float32)
    normed = (gathered_wide * row_scale(gathered_wide) * mix_gain).astype(jnp.bfloat16)
    gate_part = matmul(normed, gate_proj).astype(jnp.bfloat16)
    input_part = matmul(normed, input_proj).astype(jnp.bfloat16)
    write_part = matmul(normed, write_proj).astype(jnp.bfloat16)
    read_part = matmul(normed, read_proj).astype(jnp.bfloat16)
    gate_rows, input_rows, write_rows, read_rows = (
        lax.all_to_all(gate_part, "ep", split_axis=0, concat_axis=1, tiled=True),
        lax.all_to_all(input_part, "ep", split_axis=0, concat_axis=1, tiled=True),
        lax.all_to_all(write_part, "ep", split_axis=0, concat_axis=1, tiled=True),
        lax.all_to_all(read_part, "ep", split_axis=0, concat_axis=1, tiled=True),
    )
    normed_local = lax.dynamic_slice_in_dim(normed, device_index * local_rows, local_rows, 0)
    step_raw = matmul(normed_local, step_proj)
    inner_width = gate_rows.shape[1]
    state_span = GROUPS * STATE
    head_count = step_bias.shape[0]
    per_group = head_count // GROUPS
    fresh_row = jnp.concatenate([input_rows, write_rows, read_rows], axis=1)
    window = jnp.concatenate([conv_window, fresh_row[:, None, :]], axis=1)
    convolved = jax.nn.silu(
        jnp.sum(window.astype(jnp.float32) * conv_taps.astype(jnp.float32)[None], axis=1)
        + conv_bias
    )
    head_input = convolved[:, :inner_width].reshape(local_rows, GROUPS, per_group, HEAD_DIM)
    write_vec = convolved[:, inner_width : inner_width + state_span].reshape(
        local_rows, GROUPS, STATE
    )
    read_vec = convolved[:, inner_width + state_span :].reshape(local_rows, GROUPS, STATE)
    step_size = jax.nn.softplus(step_raw + step_bias)
    decay_rate = jnp.exp(decay_shift - step_size * jnp.exp(decay_log)).reshape(
        local_rows, GROUPS, per_group
    )
    step_group = step_size.reshape(local_rows, GROUPS, per_group)
    carried = ssm_state.reshape(local_rows, GROUPS, per_group, HEAD_DIM, STATE)
    next_state = (
        decay_rate[..., None, None] * carried
        + (step_group[..., None] * head_input)[..., None] * write_vec[:, :, None, None, :]
    )
    mixed_out = jnp.einsum("sgepn,sgn->sgep", next_state, read_vec, precision=lax.Precision.HIGHEST)
    mixed_out = mixed_out + skip_scale.reshape(GROUPS, per_group)[None, :, :, None] * head_input
    mixed_out = mixed_out.reshape(local_rows, inner_width).astype(jnp.bfloat16)
    gated_out = mixed_out.astype(jnp.float32) * jax.nn.silu(gate_rows.astype(jnp.float32))
    blocks = gated_out.reshape(local_rows, GROUPS, -1)
    gated_out = ((blocks * row_scale(blocks)).reshape(local_rows, inner_width) * group_gain).astype(
        jnp.bfloat16
    )
    col_width = out_proj.shape[1]
    resid_cols = lax.dynamic_slice_in_dim(gathered_wide, device_index * col_width, col_width, 1)
    resid_part = (
        resid_cols + matmul(lax.all_gather(gated_out, "ep", axis=0, tiled=True), out_proj)
    ).astype(jnp.bfloat16)
    gain_part = lax.dynamic_slice_in_dim(ffn_gain, device_index * col_width, col_width, 0)
    shared_part = (resid_part.astype(jnp.float32) * gain_part).astype(jnp.bfloat16)
    shared_pre = lax.psum_scatter(
        jnp.concatenate(
            [matmul(shared_part, shared_gate), matmul(shared_part, shared_up)], axis=1
        ).astype(jnp.bfloat16),
        "ep",
        scatter_dimension=0,
        tiled=True,
    ).astype(jnp.float32)
    exp_dev = expert_gate.shape[0]
    resid = lax.all_to_all(resid_part, "ep", split_axis=0, concat_axis=1, tiled=True)
    resid_wide = resid.astype(jnp.float32)
    norm_scale = row_scale(resid_wide)
    routed_in = (resid_wide * norm_scale * ffn_gain).astype(jnp.bfloat16)
    weights = route_weights(routed_in, router, expert_ids)
    expert_total = router.shape[1]
    member = jnp.any(
        expert_ids[:, :, None] == jnp.arange(expert_total, dtype=jnp.int32)[None, None, :], axis=1
    ).astype(jnp.int32)
    earlier = jnp.cumsum(member, axis=0) - member
    slot_index = jnp.take_along_axis(earlier, expert_ids, axis=1)
    places = expert_ids * CAP + slot_index
    dispatch_table = jnp.any(
        places[None, :, :] == jnp.arange(expert_total * CAP, dtype=jnp.int32)[:, None, None], axis=2
    ).astype(jnp.bfloat16)
    outbound = (
        matmul(dispatch_table, routed_in)
        .astype(jnp.bfloat16)
        .reshape(lax.axis_size("ep"), exp_dev, CAP, routed_in.shape[1])
    )
    arrived = lax.all_to_all(outbound, "ep", split_axis=0, concat_axis=0, tiled=True)
    rows_in = arrived[:, 0].reshape(-1, arrived.shape[-1])
    result = expert_result(rows_in, expert_gate[0], expert_up[0], expert_down[0])
    results = [result.reshape(arrived.shape[0], arrived.shape[2], arrived.shape[3])]
    returned = lax.all_to_all(
        jnp.stack(results, axis=1), "ep", split_axis=0, concat_axis=0, tiled=True
    )
    returned_flat = returned.reshape(expert_total * CAP, returned.shape[-1])
    picked = jnp.take(returned_flat, places.reshape(-1), axis=0).reshape(
        local_rows, expert_ids.shape[1], returned.shape[-1]
    )
    routed = jnp.sum(picked.astype(jnp.float32) * weights[:, :, None], axis=1)
    hidden_units = shared_down.shape[0]
    shared_hidden = (
        jax.nn.silu(norm_scale * shared_pre[:, :hidden_units])
        * (norm_scale * shared_pre[:, hidden_units:])
    ).astype(jnp.bfloat16)
    layer_out = (resid_wide + routed + matmul(shared_hidden, shared_down)).astype(jnp.bfloat16)
    return (layer_out, next_state.reshape(ssm_state.shape), window[:, 1:])


def solution(mesh):
    placed = (
        P(("grp", "ep"), None),
        P(("grp", "ep"), None, None),
        P(("grp", "ep"), None, None, None),
        P(None, "ep"),
        P(None, "ep"),
        P(None, "ep"),
        P(None, "ep"),
        P(),
        P(),
        P(),
        P(("grp", "ep"), None),
        P(),
        P(),
        P(),
        P(),
        P(),
        P(None, "ep"),
        P(),
        P(),
        P(("grp", "ep"), None),
        P("ep", None, None),
        P("ep", None, None),
        P("ep", None, None),
        P("ep", None),
        P("ep", None),
        P(),
    )
    return jax.shard_map(
        shards,
        mesh=mesh,
        in_specs=placed,
        out_specs=(
            P(("grp", "ep"), None),
            P(("grp", "ep"), None, None, None),
            P(("grp", "ep"), None, None),
        ),
        check_vma=False,
    )
```

profile of v0, /device:TPU:0, one launch (start us, length us, event | category | flops | bytes accessed | tf_op | source)
XLA Modules:
  0.0 219.6 jit_solution(2211372966477305906)
XLA Ops:
  7.3 24.2 %all-gather = bf16[16,3,2048]{2,1,0:T(4,128)(2,1)S(1)} all-gather(bf16[1,3,2048]{2,1,0:T(4,128)(2,1)} %bitcast.106), channel_id=1, replica_groups=mesh['grp'=2,'ep'=16] {'ep'}, dimensions={0}, use_global_device_ids=true | all-gather | bytes 208896 | tf_op jit(solution)/shard_map/all_gather | solution.py:65
  32.6 1.2 convolution_convert_fusion.7
  34.4 3.5 %all-to-all-start.1 = ((bf16[16,3,64]{2,1,0:T(4,128)(2,1)}), bf16[16,3,64]{2,1,0:T(4,128)(2,1)S(1)}, u32[]{:S(2)}, u32[]{:S(2)}) async-start(bf16[16,3,64]{2,1,0:T(4,128)(2,1)} %all_to_all.72), calls=%async_computation.1 | async-start | bytes 32768 | tf_op jit(solution)/shard_map/all_to_all | solution.py:75
  39.4 1.5 convolution_convert_fusion.5
  40.9 1.2 convolution_convert_fusion.6
  42.7 1.5 convolution_convert_fusion.4
  46.3 6.0 %all-to-all-start.2 = ((bf16[16,3,64]{2,1,0:T(4,128)(2,1)}), bf16[16,3,64]{2,1,0:T(4,128)(2,1)S(1)}, u32[]{:S(2)}, u32[]{:S(2)}) async-start(bf16[16,3,64]{2,1,0:T(4,128)(2,1)} %all_to_all.76), calls=%async_computation.2 | async-start | bytes 32768 | tf_op jit(solution)/shard_map/all_to_all | solution.py:76
  53.0 5.8 %all-to-all-done.2 = bf16[16,3,64]{2,1,0:T(4,128)(2,1)S(1)} async-done(((bf16[16,3,64]{2,1,0:T(4,128)(2,1)}), bf16[16,3,64]{2,1,0:T(4,128)(2,1)S(1)}, u32[]{:S(2)}, u32[]{:S(2)}) %all-to-all-start.2) | async-done | bytes 6176 | tf_op jit(solution)/shard_map/all_to_all | solution.py:76
  58.7 3.5 %all-to-all-start = ((bf16[16,3,256]{2,1,0:T(4,128)(2,1)}), bf16[16,3,256]{2,1,0:T(4,128)(2,1)S(1)}, u32[]{:S(2)}, u32[]{:S(2)}) async-start(bf16[16,3,256]{2,1,0:T(4,128)(2,1)} %all_to_all.68), calls=%async_computation | async-start | bytes 65536 | tf_op jit(solution)/shard_map/all_to_all | solution.py:74
  64.7 4.2 %all-to-all-done = bf16[16,3,256]{2,1,0:T(4,128)(2,1)S(1)} async-done(((bf16[16,3,256]{2,1,0:T(4,128)(2,1)}), bf16[16,3,256]{2,1,0:T(4,128)(2,1)S(1)}, u32[]{:S(2)}, u32[]{:S(2)}) %all-to-all-start) | async-done | bytes 24608 | tf_op jit(solution)/shard_map/all_to_all | solution.py:74
  68.9 3.5 %all-to-all-start.3 = ((bf16[16,3,256]{2,1,0:T(4,128)(2,1)}), bf16[16,3,256]{2,1,0:T(4,128)(2,1)S(1)}, u32[]{:S(2)}, u32[]{:S(2)}) async-start(bf16[16,3,256]{2,1,0:T(4,128)(2,1)} %all_to_all.80), calls=%async_computation.3 | async-start | bytes 65536 | tf_op jit(solution)/shard_map/all_to_all | solution.py:73
  74.7 4.2 %all-to-all-done.3 = bf16[16,3,256]{2,1,0:T(4,128)(2,1)S(1)} async-done(((bf16[16,3,256]{2,1,0:T(4,128)(2,1)}), bf16[16,3,256]{2,1,0:T(4,128)(2,1)S(1)}, u32[]{:S(2)}, u32[]{:S(2)}) %all-to-all-start.3) | async-done | bytes 24608 | tf_op jit(solution)/shard_map/all_to_all | solution.py:73
  79.2 16.8 %fusion = f32[3,8,1,8,64]{4,2,3,1,0:T(1,128)S(1)} fusion(f32[3,8,128,1,1]{2,3,4,1,0:T(1,128)S(1)} %bitcast.105, f32[3,8,8,64,128]{4,3,2,1,0:T(8,128)} %bitcast.96, f32[3,8,128]{2,1,0:T(8,128)S(1)} %bitcast.102, f32[3,8,8,64]{3,2,1,0:T(8,128)S(1)} %broadcast_multiply_fusion.1, f32[3,8,8]{2,1,0:T(8,128)S(1)} %mul.238), kind=kOutput, calls=%fused_computation.4 | convolution fusion | flops 23592960 | bytes 6415104 | tf_op jit(solution)/shard_map/sgepn,sgn->sgep/dot_general | solution.py:105
  96.5 19.0 %all-gather.1 = bf16[16,3,4096]{2,1,0:T(4,128)(2,1)S(1)} all-gather(bf16[1,3,4096]{2,1,0:T(4,128)(2,1)S(1)} %fusion.40), channel_id=1, replica_groups=mesh['grp'=2,'ep'=16] {'ep'}, dimensions={0}, use_global_device_ids=true | all-gather | bytes 417792 | tf_op jit(solution)/shard_map/all_gather | solution.py:116
  115.9 1.5 fusion.21
  120.8 3.5 %all-to-all-start.4 = ((bf16[16,3,128]{2,1,0:T(4,128)(2,1)}), bf16[16,3,128]{2,1,0:T(4,128)(2,1)S(1)}, u32[]{:S(2)}, u32[]{:S(2)}) async-start(bf16[16,3,128]{2,1,0:T(4,128)(2,1)} %all_to_all.82), calls=%async_computation.4 | async-start | bytes 32768 | tf_op jit(solution)/shard_map/all_to_all | solution.py:129
  125.3 7.0 %multiply_add_fusion = f32[3,64,64,128]{3,2,1,0:T(8,128)} fusion(f32[3,64,64,128]{3,2,1,0:T(8,128)} %param.28, f32[3,64,128]{2,1,0:T(8,128)S(1)} %broadcast_bitcast_fusion, f32[3,64,64]{2,1,0:T(8,128)S(1)} %broadcast_multiply_fusion, f32[3,64]{1,0:T(4,128)S(1)} %get-tuple-element.11), kind=kLoop, calls=%fused_computation.3 | loop fusion | flops 4718592 | bytes 12731136 | tf_op jit(solution)/shard_map/add | solution.py:102
  133.4 6.0 %all-to-all-start.5 = ((bf16[16,1,2,2048]{3,2,1,0:T(2,128)(2,1)}), bf16[16,1,2,2048]{3,2,1,0:T(2,128)(2,1)S(1)}, u32[]{:S(2)}, u32[]{:S(2)}) async-start(bf16[16,1,2,2048]{3,2,1,0:T(2,128)(2,1)} %bitcast.18), calls=%async_computation.5 | async-start | bytes 262144 | tf_op jit(solution)/shard_map/all_to_all | solution.py:149
  140.7 6.7 %all-to-all-done.5 = bf16[16,1,2,2048]{3,2,1,0:T(2,128)(2,1)S(1)} async-done(((bf16[16,1,2,2048]{3,2,1,0:T(2,128)(2,1)}), bf16[16,1,2,2048]{3,2,1,0:T(2,128)(2,1)S(1)}, u32[]{:S(2)}, u32[]{:S(2)}) %all-to-all-start.5) | async-done | bytes 131104 | tf_op jit(solution)/shard_map/all_to_all | solution.py:149
  147.4 2.0 fusion.11
  149.4 2.5 %convolution_convert_fusion = bf16[32,2048]{1,0:T(8,128)(2,1)S(1)} fusion(bf16[1,512,2048]{2,1,0:T(8,128)(2,1)S(1)} %copy-done, bf16[32,2048]{1,0:T(8,128)(2,1)S(1)} %reshape_squeeze.3, bf16[1,2048,512]{2,1,0:T(8,128)(2,1)} %param.47, f32[32,512]{1,0:T(8,128)S(1)} %fusion.11), kind=kOutput, calls=%fused_computation.11 | convolution fusion | flops 134381568 | bytes 4521984 | tf_op jit(solution)/shard_map/dot_general | solution.py:19
  152.7 3.5 %all-to-all-start.6 = ((bf16[16,1,2,2048]{3,2,1,0:T(2,128)(2,1)}), bf16[16,1,2,2048]{3,2,1,0:T(2,128)(2,1)S(1)}, u32[]{:S(2)}, u32[]{:S(2)}) async-start(bf16[16,1,2,2048]{3,2,1,0:T(2,128)(2,1)} %bitcast.22), calls=%async_computation.6 | async-start | bytes 262144 | tf_op jit(solution)/shard_map/all_to_all | solution.py:153
  156.3 52.1 %all-reduce.3.cloned.1.call-done = bf16[48,1024]{1,0:T(8,128)(2,1)} async-done(((bf16[48,1024]{1,0:T(8,128)(2,1)}), bf16[48,1024]{1,0:T(8,128)(2,1)}) %all-reduce.3.cloned.1.call-update) | async-done | bytes 98320
  210.1 2.6 %fusion.7 = bf16[3,2048]{1,0:T(4,128)(2,1)} fusion(bf16[512,2048]{1,0:T(8,128)(2,1)} %param.51, f32[3,2048]{1,0:T(4,128)S(1)} %multiply_reduce_fusion.2, bf16[16,3,128]{2,1,0:T(4,128)(2,1)S(1)} %all-to-all-done.4, f32[3,1024]{1,0:T(4,128)S(1)} %dynamic-slice_convert_fusion, f32[3]{0:T(128)S(1)} %add_rsqrt_fusion.1), kind=kOutput, calls=%fused_computation.14 | convolution fusion | flops 6328320 | bytes 2158604 | tf_op jit(solution)/shard_map/dot_general | solution.py:19
  (108 shorter events, 20.9 us)
Async XLA Ops:
  7.2 142.3 %copy-start = (bf16[1,512,2048]{2,1,0:T(8,128)(2,1)S(1)}, bf16[1,512,2048]{2,1,0:T(8,128)(2,1)}, u32[]{:S(2)}) copy-start(bf16[1,512,2048]{2,1,0:T(8,128)(2,1)} %param.48) | copy-start | bytes 6291460
  7.2 56.1 %copy-start.12 = (u32[32]{0:T(128)S(1)}, u32[32]{0:T(128)}, u32[]{:S(2)}) copy-start(u32[32]{0:T(128)} %constant.128) | copy-start | bytes 388
  7.2 38.1 %copy-start.3 = (s32[3,6]{1,0:T(4,128)S(1)}, s32[3,6]{1,0:T(4,128)}, u32[]{:S(2)}) copy-start(s32[3,6]{1,0:T(4,128)} %param.45) | copy-start | bytes 220
  7.2 38.2 %copy-start.2 = (bf16[2048,64]{0,1:T(8,128)(2,1)S(1)}, bf16[2048,64]{0,1:T(8,128)(2,1)}, u32[]{:S(2)}) copy-start(bf16[2048,64]{0,1:T(8,128)(2,1)} %param.33) | copy-start | bytes 786436
  7.2 38.2 %copy-start.9 = (f32[64]{0:T(128)S(1)}, f32[64]{0:T(128)}, u32[]{:S(2)}) copy-start(f32[64]{0:T(128)} %param.34) | copy-start | bytes 772
  7.2 38.2 %copy-start.8 = (f32[3,64]{1,0:T(4,128)S(1)}, f32[3,64]{1,0:T(4,128)}, u32[]{:S(2)}) copy-start(f32[3,64]{1,0:T(4,128)} %param.36) | copy-start | bytes 2308
  7.2 55.0 %copy-start.4 = (bf16[4,6144]{1,0:T(4,128)(2,1)S(1)}, bf16[4,6144]{1,0:T(4,128)(2,1)}, u32[]{:S(2)}) copy-start(bf16[4,6144]{1,0:T(4,128)(2,1)} %param.38) | copy-start | bytes 147460
  7.2 55.8 %copy-start.10 = (f32[64]{0:T(128)S(1)}, f32[64]{0:T(128)}, u32[]{:S(2)}) copy-start(f32[64]{0:T(128)} %param.37) | copy-start | bytes 772
  7.3 55.9 %copy-start.7 = (f32[2048]{0:T(1024)S(1)}, f32[2048]{0:T(1024)}, u32[]{:S(2)}) copy-start(f32[2048]{0:T(1024)} %param.43) | copy-start | bytes 24580
  7.3 65.2 %copy-start.1 = (bf16[3,3,6144]{2,1,0:T(4,128)(2,1)S(1)}, bf16[3,3,6144]{2,1,0:T(4,128)(2,1)}, u32[]{:S(2)}) copy-start(bf16[3,3,6144]{2,1,0:T(4,128)(2,1)} %param.27) | copy-start | bytes 331780
  7.3 66.4 %copy-start.5 = (f32[6144]{0:T(1024)S(1)}, f32[6144]{0:T(1024)}, u32[]{:S(2)}) copy-start(f32[6144]{0:T(1024)} %param.39) | copy-start | bytes 73732
  34.4 11.9 %all-to-all-start.1 = ((bf16[16,3,64]{2,1,0:T(4,128)(2,1)}), bf16[16,3,64]{2,1,0:T(4,128)(2,1)S(1)}, u32[]{:S(2)}, u32[]{:S(2)}) async-start(bf16[16,3,64]{2,1,0:T(4,128)(2,1)} %all_to_all.72), calls=%async_computation.1 | async-start | bytes 32768 | tf_op jit(solution)/shard_map/all_to_all | solution.py:75
  44.4 52.0 %copy-start.6 = (f32[4096]{0:T(1024)S(1)}, f32[4096]{0:T(1024)}, u32[]{:S(2)}) copy-start(f32[4096]{0:T(1024)} %param.41) | copy-start | bytes 49156
  46.3 12.5 %all-to-all-start.2 = ((bf16[16,3,64]{2,1,0:T(4,128)(2,1)}), bf16[16,3,64]{2,1,0:T(4,128)(2,1)S(1)}, u32[]{:S(2)}, u32[]{:S(2)}) async-start(bf16[16,3,64]{2,1,0:T(4,128)(2,1)} %all_to_all.76), calls=%async_computation.2 | async-start | bytes 32768 | tf_op jit(solution)/shard_map/all_to_all | solution.py:76
  58.7 10.1 %all-to-all-start = ((bf16[16,3,256]{2,1,0:T(4,128)(2,1)}), bf16[16,3,256]{2,1,0:T(4,128)(2,1)S(1)}, u32[]{:S(2)}, u32[]{:S(2)}) async-start(bf16[16,3,256]{2,1,0:T(4,128)(2,1)} %all_to_all.68), calls=%async_computation | async-start | bytes 65536 | tf_op jit(solution)/shard_map/all_to_all | solution.py:74
  68.9 10.1 %all-to-all-start.3 = ((bf16[16,3,256]{2,1,0:T(4,128)(2,1)}), bf16[16,3,256]{2,1,0:T(4,128)(2,1)S(1)}, u32[]{:S(2)}, u32[]{:S(2)}) async-start(bf16[16,3,256]{2,1,0:T(4,128)(2,1)} %all_to_all.80), calls=%async_computation.3 | async-start | bytes 65536 | tf_op jit(solution)/shard_map/all_to_all | solution.py:73
  72.4 136.1 %all-reduce.3.cloned.1.call-start = ((), (), s32[]{:S(2)}) async-start(), calls=%async_computation.7 | async-start | bytes 196608
  120.8 11.5 %all-to-all-start.4 = ((bf16[16,3,128]{2,1,0:T(4,128)(2,1)}), bf16[16,3,128]{2,1,0:T(4,128)(2,1)S(1)}, u32[]{:S(2)}, u32[]{:S(2)}) async-start(bf16[16,3,128]{2,1,0:T(4,128)(2,1)} %all_to_all.82), calls=%async_computation.4 | async-start | bytes 32768 | tf_op jit(solution)/shard_map/all_to_all | solution.py:129
  125.3 14.1 %copy-start.11 = (bf16[2048,16]{0,1:T(8,128)(2,1)S(1)}, bf16[2048,16]{0,1:T(8,128)(2,1)}, u32[]{:S(2)}) copy-start(bf16[2048,16]{0,1:T(8,128)(2,1)} %param.44) | copy-start | bytes 196612
  133.4 13.9 %all-to-all-start.5 = ((bf16[16,1,2,2048]{3,2,1,0:T(2,128)(2,1)}), bf16[16,1,2,2048]{3,2,1,0:T(2,128)(2,1)S(1)}, u32[]{:S(2)}, u32[]{:S(2)}) async-start(bf16[16,1,2,2048]{3,2,1,0:T(2,128)(2,1)} %bitcast.18), calls=%async_computation.5 | async-start | bytes 262144 | tf_op jit(solution)/shard_map/all_to_all | solution.py:149
  152.7 56.5 %all-to-all-start.6 = ((bf16[16,1,2,2048]{3,2,1,0:T(2,128)(2,1)}), bf16[16,1,2,2048]{3,2,1,0:T(2,128)(2,1)S(1)}, u32[]{:S(2)}, u32[]{:S(2)}) async-start(bf16[16,1,2,2048]{3,2,1,0:T(2,128)(2,1)} %bitcast.22), calls=%async_computation.6 | async-start | bytes 262144 | tf_op jit(solution)/shard_map/all_to_all | solution.py:153
Sparse Core Ops, SparseCore 0:
  120.9 87.4 all-reduce.2
where the time goes:
time: 221 us; the launch traced here: 220 us
  waiting for transfers between devices  73 us (33%)
  blocking collectives  43.3 us (20%)
  matrix products  33.5 us (15%)
  starting transfers between devices  29.5 us (13%)
  between operations  15.2 us (7%)
  other arithmetic  14.1 us (6%)
  local copies, waits for them, and re-layouts  11 us (5%)
    unnamed x2, waiting for transfers between devices  52.2 us
    all_gather x1, blocking collectives, shards(): gathered = lax.all_gather(hidden, 'ep', axis=0, tiled=True)  24.2 us
    all_gather x1, blocking collectives, shards(): lax.all_gather(gated_out, 'ep', axis=0, tiled=True)  19 us
    dot_general x13, matrix products, matmul(): return jnp.dot(left, right, preferred_element_type=jnp.float32)  16.8 us
    dot_general x1, matrix products, shards(): jnp.einsum('sgepn,sgn->sgep', next_state, read_vec, precision=lax.Precisi...  16.8 us
    add x1, other arithmetic, shards(): decay_rate[..., None, None] * carried  6.99 us
    all_to_all x1, waiting for transfers between devices, shards(): lax.all_to_all(outbound, 'ep', split_axis=0, concat_axis=0, tiled=True)  6.66 us
    all_to_all x1, starting transfers between devices, shards(): lax.all_to_all(read_part, 'ep', split_axis=0, concat_axis=1, tiled=True)  5.97 us
  transfers between devices with their start and end apart: 8, of which 5 were waited for; matrix products, arithmetic and copies ran while one was open for 13% of the time, Pallas kernels for 0%

commit v1 on v0

--- a/solution.py
+++ b/solution.py
@@ -73,7 +73,12 @@
         lax.all_to_all(gate_part, "ep", split_axis=0, concat_axis=1, tiled=True),
         lax.all_to_all(input_part, "ep", split_axis=0, concat_axis=1, tiled=True),
         lax.all_to_all(write_part, "ep", split_axis=0, concat_axis=1, tiled=True),
-        lax.all_to_all(read_part, "ep", split_axis=0, concat_axis=1, tiled=True),
+        jnp.concatenate(
+            lax.all_to_all(
+                jnp.stack(jnp.split(read_part, lax.axis_size("ep"), axis=0)), "ep", 0, 0
+            ),
+            axis=1,
+        ),
     )
     normed_local = lax.dynamic_slice_in_dim(normed, device_index * local_rows, local_rows, 0)
     step_raw = matmul(normed_local, step_proj)

time: 221 us -> 237 us (1.072)
  local copies, waits for them, and re-layouts: 11 us -> 19.4 us
  waiting for transfers between devices: 73 us -> 80.8 us
    unnamed x33 -> x48, local copies, waits for them, and re-layouts: 1.12 us -> 9.61 us
    unnamed x2, waiting for transfers between devices: 52.2 us -> 59.8 us
    all_to_all x1, waiting for transfers between devices: 0.01 us -> 5.78 us  [shards(): lax.all_to_all(write_part, 'ep', split_axis=0, concat_axis=1, tiled=True)]
    all_to_all x1, waiting for transfers between devices: 5.78 us -> 0.01 us  [shards(): lax.all_to_all(jnp.stack(jnp.split(read_part, lax.axis_size('ep'), axis=0...]
    all_to_all x1, starting transfers between devices: 5.97 us -> 3.49 us  [shards(): lax.all_to_all(jnp.stack(jnp.split(read_part, lax.axis_size('ep'), axis=0...]
    all_to_all x1, starting transfers between devices: 3.49 us -> 5.97 us  [shards(): lax.all_to_all(write_part, 'ep', split_axis=0, concat_axis=1, tiled=True)]
where the time goes in v1:
time: 237 us; the launch traced here: 236 us
  waiting for transfers between devices  80.8 us (34%)
  blocking collectives  43.3 us (18%)
  matrix products  33.6 us (14%)
  starting transfers between devices  29.5 us (12%)
  local copies, waits for them, and re-layouts  19.4 us (8%)
  between operations  15.2 us (6%)
  other arithmetic  14.1 us (6%)
    unnamed x2, waiting for transfers between devices  59.8 us
    all_gather x1, blocking collectives, shards(): gathered = lax.all_gather(hidden, 'ep', axis=0, tiled=True)  24.2 us
    all_gather x1, blocking collectives, shards(): lax.all_gather(gated_out, 'ep', axis=0, tiled=True)  19 us
    dot_general x13, matrix products, matmul(): return jnp.dot(left, right, preferred_element_type=jnp.float32)  16.8 us
    dot_general x1, matrix products, shards(): jnp.einsum('sgepn,sgn->sgep', next_state, read_vec, precision=lax.Precisi...  16.8 us
    unnamed x48, local copies, waits for them, and re-layouts  9.61 us
    add x1, other arithmetic, shards(): decay_rate[..., None, None] * carried  6.99 us
    all_to_all x1, waiting for transfers between devices, shards(): lax.all_to_all(outbound, 'ep', split_axis=0, concat_axis=0, tiled=True)  6.71 us
  transfers between devices with their start and end apart: 8, of which 5 were waited for; matrix products, arithmetic and copies ran while one was open for 13% of the time, Pallas kernels for 0%

profile of v1, /device:TPU:0, one launch (start us, length us, event | category | flops | bytes accessed | tf_op | source)
XLA Modules:
  0.0 235.7 jit_solution(10095147501864933205)
XLA Ops:
  7.3 24.2 %all-gather = bf16[16,3,2048]{2,1,0:T(4,128)(2,1)S(1)} all-gather(bf16[1,3,2048]{2,1,0:T(4,128)(2,1)} %bitcast.170), channel_id=1, replica_groups=mesh['grp'=2,'ep'=16] {'ep'}, dimensions={0}, use_global_device_ids=true | all-gather | bytes 208896 | tf_op jit(solution)/shard_map/all_gather | solution.py:65
  32.6 1.2 convolution_convert_fusion.6
  42.8 3.5 %all-to-all-start.2 = ((bf16[16,3,64]{2,1,0:T(4,128)(2,1)}), bf16[16,3,64]{2,1,0:T(4,128)(2,1)S(1)}, u32[]{:S(2)}, u32[]{:S(2)}) async-start(bf16[16,3,64]{2,1,0:T(4,128)(2,1)} %constant_dynamic-update-slice_fusion), calls=%async_computation.2 | async-start | bytes 32768 | tf_op jit(solution)/shard_map/all_to_all | solution.py:77
  47.8 1.5 convolution_convert_fusion.4
  49.3 1.2 convolution_convert_fusion.7
  50.5 1.5 convolution_convert_fusion.5
  54.7 6.0 %all-to-all-start.1 = ((bf16[16,3,64]{2,1,0:T(4,128)(2,1)}), bf16[16,3,64]{2,1,0:T(4,128)(2,1)S(1)}, u32[]{:S(2)}, u32[]{:S(2)}) async-start(bf16[16,3,64]{2,1,0:T(4,128)(2,1)} %all_to_all.61), calls=%async_computation.1 | async-start | bytes 32768 | tf_op jit(solution)/shard_map/all_to_all | solution.py:75
  61.4 5.8 %all-to-all-done.1 = bf16[16,3,64]{2,1,0:T(4,128)(2,1)S(1)} async-done(((bf16[16,3,64]{2,1,0:T(4,128)(2,1)}), bf16[16,3,64]{2,1,0:T(4,128)(2,1)S(1)}, u32[]{:S(2)}, u32[]{:S(2)}) %all-to-all-start.1) | async-done | bytes 6176 | tf_op jit(solution)/shard_map/all_to_all | solution.py:75
  67.2 3.5 %all-to-all-start = ((bf16[16,3,256]{2,1,0:T(4,128)(2,1)}), bf16[16,3,256]{2,1,0:T(4,128)(2,1)S(1)}, u32[]{:S(2)}, u32[]{:S(2)}) async-start(bf16[16,3,256]{2,1,0:T(4,128)(2,1)} %all_to_all.57), calls=%async_computation | async-start | bytes 65536 | tf_op jit(solution)/shard_map/all_to_all | solution.py:74
  73.1 4.2 %all-to-all-done = bf16[16,3,256]{2,1,0:T(4,128)(2,1)S(1)} async-done(((bf16[16,3,256]{2,1,0:T(4,128)(2,1)}), bf16[16,3,256]{2,1,0:T(4,128)(2,1)S(1)}, u32[]{:S(2)}, u32[]{:S(2)}) %all-to-all-start) | async-done | bytes 24608 | tf_op jit(solution)/shard_map/all_to_all | solution.py:74
  77.3 3.5 %all-to-all-start.3 = ((bf16[16,3,256]{2,1,0:T(4,128)(2,1)}), bf16[16,3,256]{2,1,0:T(4,128)(2,1)S(1)}, u32[]{:S(2)}, u32[]{:S(2)}) async-start(bf16[16,3,256]{2,1,0:T(4,128)(2,1)} %all_to_all.66), calls=%async_computation.3 | async-start | bytes 65536 | tf_op jit(solution)/shard_map/all_to_all | solution.py:73
  83.1 4.3 %all-to-all-done.3 = bf16[16,3,256]{2,1,0:T(4,128)(2,1)S(1)} async-done(((bf16[16,3,256]{2,1,0:T(4,128)(2,1)}), bf16[16,3,256]{2,1,0:T(4,128)(2,1)S(1)}, u32[]{:S(2)}, u32[]{:S(2)}) %all-to-all-start.3) | async-done | bytes 24608 | tf_op jit(solution)/shard_map/all_to_all | solution.py:73
  87.6 16.8 %fusion = f32[3,8,1,8,64]{4,2,3,1,0:T(1,128)S(1)} fusion(f32[3,8,128,1,1]{2,3,4,1,0:T(1,128)S(1)} %bitcast.169, f32[3,8,8,64,128]{4,3,2,1,0:T(8,128)} %bitcast.160, f32[3,8,128]{2,1,0:T(8,128)S(1)} %bitcast.166, f32[3,8,8,64]{3,2,1,0:T(8,128)S(1)} %broadcast_multiply_fusion.1, f32[3,8,8]{2,1,0:T(8,128)S(1)} %mul.238), kind=kOutput, calls=%fused_computation.4 | convolution fusion | flops 23592960 | bytes 6415104 | tf_op jit(solution)/shard_map/sgepn,sgn->sgep/dot_general | solution.py:110
  104.9 19.0 %all-gather.1 = bf16[16,3,4096]{2,1,0:T(4,128)(2,1)S(1)} all-gather(bf16[1,3,4096]{2,1,0:T(4,128)(2,1)S(1)} %fusion.40), channel_id=1, replica_groups=mesh['grp'=2,'ep'=16] {'ep'}, dimensions={0}, use_global_device_ids=true | all-gather | bytes 417792 | tf_op jit(solution)/shard_map/all_gather | solution.py:121
  124.3 1.5 fusion.21
  126.5 3.5 %all-to-all-start.4 = ((bf16[16,3,128]{2,1,0:T(4,128)(2,1)}), bf16[16,3,128]{2,1,0:T(4,128)(2,1)S(1)}, u32[]{:S(2)}, u32[]{:S(2)}) async-start(bf16[16,3,128]{2,1,0:T(4,128)(2,1)} %all_to_all.68), calls=%async_computation.4 | async-start | bytes 32768 | tf_op jit(solution)/shard_map/all_to_all | solution.py:134
  133.8 7.0 %multiply_add_fusion = f32[3,64,64,128]{3,2,1,0:T(8,128)} fusion(f32[3,64,64,128]{3,2,1,0:T(8,128)} %param.28, f32[3,64,128]{2,1,0:T(8,128)S(1)} %broadcast_bitcast_fusion, f32[3,64,64]{2,1,0:T(8,128)S(1)} %broadcast_multiply_fusion, f32[3,64]{1,0:T(4,128)S(1)} %get-tuple-element.11), kind=kLoop, calls=%fused_computation.3 | loop fusion | flops 4718592 | bytes 12731136 | tf_op jit(solution)/shard_map/add | solution.py:107
  141.9 6.0 %all-to-all-start.5 = ((bf16[16,1,2,2048]{3,2,1,0:T(2,128)(2,1)}), bf16[16,1,2,2048]{3,2,1,0:T(2,128)(2,1)S(1)}, u32[]{:S(2)}, u32[]{:S(2)}) async-start(bf16[16,1,2,2048]{3,2,1,0:T(2,128)(2,1)} %bitcast.34), calls=%async_computation.5 | async-start | bytes 262144 | tf_op jit(solution)/shard_map/all_to_all | solution.py:154
  149.2 6.7 %all-to-all-done.5 = bf16[16,1,2,2048]{3,2,1,0:T(2,128)(2,1)S(1)} async-done(((bf16[16,1,2,2048]{3,2,1,0:T(2,128)(2,1)}), bf16[16,1,2,2048]{3,2,1,0:T(2,128)(2,1)S(1)}, u32[]{:S(2)}, u32[]{:S(2)}) %all-to-all-start.5) | async-done | bytes 131104 | tf_op jit(solution)/shard_map/all_to_all | solution.py:154
  155.9 2.1 fusion.11
  158.0 2.5 %convolution_convert_fusion = bf16[32,2048]{1,0:T(8,128)(2,1)S(1)} fusion(bf16[1,512,2048]{2,1,0:T(8,128)(2,1)S(1)} %copy-done, bf16[32,2048]{1,0:T(8,128)(2,1)S(1)} %reshape_squeeze.3, bf16[1,2048,512]{2,1,0:T(8,128)(2,1)} %param.47, f32[32,512]{1,0:T(8,128)S(1)} %fusion.11), kind=kOutput, calls=%fused_computation.11 | convolution fusion | flops 134381568 | bytes 4521984 | tf_op jit(solution)/shard_map/dot_general | solution.py:19
  161.3 3.5 %all-to-all-start.6 = ((bf16[16,1,2,2048]{3,2,1,0:T(2,128)(2,1)}), bf16[16,1,2,2048]{3,2,1,0:T(2,128)(2,1)S(1)}, u32[]{:S(2)}, u32[]{:S(2)}) async-start(bf16[16,1,2,2048]{3,2,1,0:T(2,128)(2,1)} %bitcast.38), calls=%async_computation.6 | async-start | bytes 262144 | tf_op jit(solution)/shard_map/all_to_all | solution.py:158
  164.9 59.8 %all-reduce.3.cloned.1.call-done = bf16[48,1024]{1,0:T(8,128)(2,1)} async-done(((bf16[48,1024]{1,0:T(8,128)(2,1)}), bf16[48,1024]{1,0:T(8,128)(2,1)}) %all-reduce.3.cloned.1.call-update) | async-done | bytes 98320
  226.3 2.6 %fusion.7 = bf16[3,2048]{1,0:T(4,128)(2,1)} fusion(bf16[512,2048]{1,0:T(8,128)(2,1)} %param.51, f32[3,2048]{1,0:T(4,128)S(1)} %multiply_reduce_fusion.2, bf16[16,3,128]{2,1,0:T(4,128)(2,1)S(1)} %all-to-all-done.4, f32[3,1024]{1,0:T(4,128)S(1)} %dynamic-slice_convert_fusion, f32[3]{0:T(128)S(1)} %add_rsqrt_fusion.1), kind=kOutput, calls=%fused_computation.14 | convolution fusion | flops 6328320 | bytes 2158604 | tf_op jit(solution)/shard_map/dot_general | solution.py:19
  (123 shorter events, 29.4 us)
Async XLA Ops:
  7.2 150.8 %copy-start = (bf16[1,512,2048]{2,1,0:T(8,128)(2,1)S(1)}, bf16[1,512,2048]{2,1,0:T(8,128)(2,1)}, u32[]{:S(2)}) copy-start(bf16[1,512,2048]{2,1,0:T(8,128)(2,1)} %param.48) | copy-start | bytes 6291460
  7.2 64.5 %copy-start.12 = (u32[32]{0:T(128)S(1)}, u32[32]{0:T(128)}, u32[]{:S(2)}) copy-start(u32[32]{0:T(128)} %constant.128) | copy-start | bytes 388
  7.2 46.6 %copy-start.3 = (s32[3,6]{1,0:T(4,128)S(1)}, s32[3,6]{1,0:T(4,128)}, u32[]{:S(2)}) copy-start(s32[3,6]{1,0:T(4,128)} %param.45) | copy-start | bytes 220
  7.2 46.6 %copy-start.8 = (f32[3,64]{1,0:T(4,128)S(1)}, f32[3,64]{1,0:T(4,128)}, u32[]{:S(2)}) copy-start(f32[3,64]{1,0:T(4,128)} %param.36) | copy-start | bytes 2308
  7.2 46.6 %copy-start.9 = (f32[64]{0:T(128)S(1)}, f32[64]{0:T(128)}, u32[]{:S(2)}) copy-start(f32[64]{0:T(128)} %param.34) | copy-start | bytes 772
  7.2 46.6 %copy-start.2 = (bf16[2048,64]{0,1:T(8,128)(2,1)S(1)}, bf16[2048,64]{0,1:T(8,128)(2,1)}, u32[]{:S(2)}) copy-start(bf16[2048,64]{0,1:T(8,128)(2,1)} %param.33) | copy-start | bytes 786436
  7.2 64.1 %copy-start.4 = (bf16[4,6144]{1,0:T(4,128)(2,1)S(1)}, bf16[4,6144]{1,0:T(4,128)(2,1)}, u32[]{:S(2)}) copy-start(bf16[4,6144]{1,0:T(4,128)(2,1)} %param.38) | copy-start | bytes 147460
  7.2 64.3 %copy-start.10 = (f32[64]{0:T(128)S(1)}, f32[64]{0:T(128)}, u32[]{:S(2)}) copy-start(f32[64]{0:T(128)} %param.37) | copy-start | bytes 772
  7.3 64.3 %copy-start.7 = (f32[2048]{0:T(1024)S(1)}, f32[2048]{0:T(1024)}, u32[]{:S(2)}) copy-start(f32[2048]{0:T(1024)} %param.43) | copy-start | bytes 24580
  7.3 73.6 %copy-start.1 = (bf16[3,3,6144]{2,1,0:T(4,128)(2,1)S(1)}, bf16[3,3,6144]{2,1,0:T(4,128)(2,1)}, u32[]{:S(2)}) copy-start(bf16[3,3,6144]{2,1,0:T(4,128)(2,1)} %param.27) | copy-start | bytes 331780
  7.3 74.8 %copy-start.5 = (f32[6144]{0:T(1024)S(1)}, f32[6144]{0:T(1024)}, u32[]{:S(2)}) copy-start(f32[6144]{0:T(1024)} %param.39) | copy-start | bytes 73732
  42.8 11.9 %all-to-all-start.2 = ((bf16[16,3,64]{2,1,0:T(4,128)(2,1)}), bf16[16,3,64]{2,1,0:T(4,128)(2,1)S(1)}, u32[]{:S(2)}, u32[]{:S(2)}) async-start(bf16[16,3,64]{2,1,0:T(4,128)(2,1)} %constant_dynamic-update-slice_fusion), calls=%async_computation.2 | async-start | bytes 32768 | tf_op jit(solution)/shard_map/all_to_all | solution.py:77
  52.8 52.0 %copy-start.6 = (f32[4096]{0:T(1024)S(1)}, f32[4096]{0:T(1024)}, u32[]{:S(2)}) copy-start(f32[4096]{0:T(1024)} %param.41) | copy-start | bytes 49156
  54.7 12.5 %all-to-all-start.1 = ((bf16[16,3,64]{2,1,0:T(4,128)(2,1)}), bf16[16,3,64]{2,1,0:T(4,128)(2,1)S(1)}, u32[]{:S(2)}, u32[]{:S(2)}) async-start(bf16[16,3,64]{2,1,0:T(4,128)(2,1)} %all_to_all.61), calls=%async_computation.1 | async-start | bytes 32768 | tf_op jit(solution)/shard_map/all_to_all | solution.py:75
  67.2 10.1 %all-to-all-start = ((bf16[16,3,256]{2,1,0:T(4,128)(2,1)}), bf16[16,3,256]{2,1,0:T(4,128)(2,1)S(1)}, u32[]{:S(2)}, u32[]{:S(2)}) async-start(bf16[16,3,256]{2,1,0:T(4,128)(2,1)} %all_to_all.57), calls=%async_computation | async-start | bytes 65536 | tf_op jit(solution)/shard_map/all_to_all | solution.py:74
  77.3 10.1 %all-to-all-start.3 = ((bf16[16,3,256]{2,1,0:T(4,128)(2,1)}), bf16[16,3,256]{2,1,0:T(4,128)(2,1)S(1)}, u32[]{:S(2)}, u32[]{:S(2)}) async-start(bf16[16,3,256]{2,1,0:T(4,128)(2,1)} %all_to_all.66), calls=%async_computation.3 | async-start | bytes 65536 | tf_op jit(solution)/shard_map/all_to_all | solution.py:73
  126.5 14.3 %all-to-all-start.4 = ((bf16[16,3,128]{2,1,0:T(4,128)(2,1)}), bf16[16,3,128]{2,1,0:T(4,128)(2,1)S(1)}, u32[]{:S(2)}, u32[]{:S(2)}) async-start(bf16[16,3,128]{2,1,0:T(4,128)(2,1)} %all_to_all.68), calls=%async_computation.4 | async-start | bytes 32768 | tf_op jit(solution)/shard_map/all_to_all | solution.py:134
  130.0 94.7 %all-reduce.3.cloned.1.call-start = ((), (), s32[]{:S(2)}) async-start(), calls=%async_computation.7 | async-start | bytes 196608
  133.8 14.1 %copy-start.11 = (bf16[2048,16]{0,1:T(8,128)(2,1)S(1)}, bf16[2048,16]{0,1:T(8,128)(2,1)}, u32[]{:S(2)}) copy-start(bf16[2048,16]{0,1:T(8,128)(2,1)} %param.44) | copy-start | bytes 196612
  141.9 14.0 %all-to-all-start.5 = ((bf16[16,1,2,2048]{3,2,1,0:T(2,128)(2,1)}), bf16[16,1,2,2048]{3,2,1,0:T(2,128)(2,1)S(1)}, u32[]{:S(2)}, u32[]{:S(2)}) async-start(bf16[16,1,2,2048]{3,2,1,0:T(2,128)(2,1)} %bitcast.34), calls=%async_computation.5 | async-start | bytes 262144 | tf_op jit(solution)/shard_map/all_to_all | solution.py:154
  161.3 64.1 %all-to-all-start.6 = ((bf16[16,1,2,2048]{3,2,1,0:T(2,128)(2,1)}), bf16[16,1,2,2048]{3,2,1,0:T(2,128)(2,1)S(1)}, u32[]{:S(2)}, u32[]{:S(2)}) async-start(bf16[16,1,2,2048]{3,2,1,0:T(2,128)(2,1)} %bitcast.38), calls=%async_computation.6 | async-start | bytes 262144 | tf_op jit(solution)/shard_map/all_to_all | solution.py:158
Sparse Core Ops, SparseCore 0:
  134.2 90.3 all-reduce.2
